TPU v7x, 32 devices: a whole 2x2x4 slice. The times are simulated.
32 devices in a mesh: sp: 4 (over y, x), tp: 8 (over z, core).
Axes of the slice: x: 2, y: 2, z: 4, core: 2. Of those that a mesh axis runs over, the one named last changes fastest.
Arguments:
- tokens: bfloat16 [8192, 2048], P('sp', 'tp'), may hold values from -6 to 6
- norm_gain: float32 [2048], replicated, may hold values from 0.1 to 1.9
- w_key: bfloat16 [2048, 1024], P(None, 'tp'), may hold values from -0.125 to 0.125
- w_decay: bfloat16 [2048, 1024], P(None, 'tp'), may hold values from -0.125 to 0.125
- w_value: bfloat16 [2048, 512], replicated, may hold values from -0.125 to 0.125
- decay_bias: float32 [1024], P('tp'), may hold values from 0 to 8.5
- gate_drift: float32 [8192], P('sp'), may hold values from -1 to 1
- queries: bfloat16 [1024], P('tp'), may hold values from -6 to 6
- out_gain: float32 [4, 512], P(None, 'sp'), may hold values from 0.1 to 1.9
Outputs:
- state_cache: bfloat16 [1024, 512], P('tp', 'sp')
- first_read: float32 [4, 512], P(None, 'sp')
All inputs are finite; a program needn't handle non-finite values.
Results may differ from a plain program's by a relative error of at most 0.009.
Values may be sent and summed in bfloat16 or wider, within the bound.
A program may use at most 128 MiB of HBM per device.

v0:
```python
import jax
import jax.numpy as jnp
from jax import lax
from jax.sharding import PartitionSpec as P

QUERY_KEY_HEADS = 4
KEY_CHANNELS = 256
VALUE_CHANNELS = 512


EPS = 1e-06
GATE_NORM = 16.0


def body(tokens, norm_gain, w_key, w_decay, w_value, decay_bias, gate_drift, queries, out_gain):
    gathered = lax.all_gather(tokens, "tp", axis=1, tiled=True)
    rows_f32 = gathered.astype(jnp.float32)
    inverse_rms = lax.rsqrt(jnp.mean(rows_f32 * rows_f32, axis=1, keepdims=True) + EPS)
    normed = (rows_f32 * inverse_rms * norm_gain[None, :]).astype(jnp.bfloat16)
    key_proj = jnp.dot(normed, w_key, preferred_element_type=jnp.float32).astype(jnp.bfloat16)
    gate_pre = jnp.dot(normed, w_decay, preferred_element_type=jnp.float32).astype(jnp.bfloat16)
    value_proj = jnp.dot(normed, w_value, preferred_element_type=jnp.float32).astype(jnp.bfloat16)
    log_decay = (
        jax.nn.log_sigmoid(gate_pre.astype(jnp.float32) + decay_bias[None, :] + gate_drift[:, None])
        / GATE_NORM
    )
    suffix = lax.cumsum(log_decay, axis=0, reverse=True)
    weighted = (key_proj.astype(jnp.float32) * jnp.exp(suffix - log_decay)).astype(jnp.bfloat16)
    partial_value = lax.dot_general(
        weighted, value_proj, (((0,), (0,)), ((), ())), preferred_element_type=jnp.float32
    )
    total_decay = suffix[0]
    channels = partial_value.shape[0]
    span_count = lax.axis_size("sp")
    spread = jnp.broadcast_to(total_decay[None, :, None], (1, channels, span_count))
    blocks, totals = (
        lax.all_to_all(partial_value[None], "sp", split_axis=2, concat_axis=0, tiled=True),
        lax.all_to_all(spread, "sp", split_axis=2, concat_axis=0, tiled=True),
    )
    later_sum = lax.cumsum(totals, axis=0, reverse=True) - totals
    matrix_state = jnp.sum(jnp.exp(later_sum) * blocks, axis=0)
    state_cache = matrix_state.astype(jnp.bfloat16)
    channel_ids = lax.axis_index("tp") * channels + jnp.arange(channels, dtype=jnp.int32)
    owners = (channel_ids // KEY_CHANNELS)[:, None] == jnp.arange(QUERY_KEY_HEADS, dtype=jnp.int32)[
        None, :
    ]
    query_of_head = jnp.where(
        owners, queries.astype(jnp.float32)[:, None] * KEY_CHANNELS ** (-0.5), 0.0
    )
    part_read = lax.dot_general(
        query_of_head, matrix_state, (((0,), (0,)), ((), ())), precision=lax.Precision.HIGHEST
    )
    summed_read = lax.psum(part_read, "tp")
    squares = lax.psum(jnp.sum(summed_read * summed_read, axis=1), "sp")
    first_read = summed_read * lax.rsqrt(squares / VALUE_CHANNELS + EPS)[:, None] * out_gain
    return (state_cache, first_read)


def solution(mesh):
    return jax.shard_map(
        body,
        mesh=mesh,
        in_specs=(
            P("sp", "tp"),
            P(),
            P(None, "tp"),
            P(None, "tp"),
            P(),
            P("tp"),
            P("sp"),
            P("tp"),
            P(None, "sp"),
        ),
        out_specs=(P("tp", "sp"), P(None, "sp")),
        check_vma=False,
    )
```

profile of v0, /device:TPU:0, one launch (start us, length us, event | category | flops | bytes accessed | tf_op | source)
XLA Modules:
  0.0 171.0 jit_solution(2722808447826279931)
XLA Ops:
  7.2 0.0 copy-start
  7.2 0.0 copy-start.5
  7.2 0.0 copy-start.3
  7.2 0.0 copy-start.6
  7.2 0.0 copy-start.4
  7.2 0.0 all-gather.2.cloned.1.call-start
  7.3 0.7 all-gather.2.cloned.1.call-update
  8.0 0.7 convert_multiply_fusion.2
  8.7 86.2 %all-gather.2.cloned.1.call-done = bf16[2048,2048]{1,0:T(8,128)(2,1)} async-done(((bf16[2048,256]{1,0:T(8,128)(2,1)}), bf16[2048,2048]{1,0:T(8,128)(2,1)}) %all-gather.2.cloned.1.call-update) | async-done | bytes 8388624 | tf_op jit(solution)/shard_map/all_gather | solution.py:16
  94.9 0.0 copy-start.1
  94.9 5.2 %fusion = f32[2048]{0:T(1024)S(1)} fusion(bf16[2048,2048]{1,0:T(8,128)(2,1)} %all-gather.2.cloned.1.call-done), kind=kLoop, calls=%fused_computation.2 | loop fusion | flops 12580864 | bytes 8396800 | tf_op jit(solution)/shard_map/reduce_sum | solution.py:18
  100.1 0.0 copy-done.5
  100.1 0.0 copy-done.3
  100.1 0.0 copy-done.6
  100.1 0.0 copy-done.4
  100.1 0.5 copy-done.1
  100.6 4.7 %fusion.12 = (f32[128,2048]{0,1:T(8,128)S(1)}, f32[2048,128]{1,0:T(8,128)}) fusion(f32[2048]{0:T(1024)S(1)} %copy-done.4, f32[128]{0:T(128)S(1)} %copy-done.6, bf16[2048,128]{1,0:T(8,128)(2,1)S(1)} %copy-done.3, bf16[2048,2048]{1,0:T(8,128)(2,1)S(1)} %copy-done.1, f32[2048]{0:T(1024)S(1)} %copy-done.5, f32[2048]{0:T(1024)S(1)} %add_rsqrt_fusion), kind=kOutput, calls=%fused_computation.19 | convolution fusion | flops 1093926912 | bytes 11035136 | tf_op jit(solution)/shard_map/dot_general | solution.py:21
  105.4 2.6 %fusion.21 = f32[128,16,128]{0,1,2:T(8,128)S(1)} fusion(f32[128,16,128]{0,2,1:T(8,128)S(1)} %bitcast.44), kind=kOutput, calls=%fused_computation.30 | output fusion | flops 33292288 | bytes 2097152 | tf_op jit(solution)/shard_map/reduce-window
  108.0 0.1 broadcast_add_fusion
  108.1 0.3 copy.17
  108.4 0.6 broadcast_in_dim.19
  109.0 3.6 %all-to-all-start = ((f32[1,128,4]{1,0,2:T(1,128)}), f32[1,128,4]{1,0,2:T(1,128)S(1)}, u32[]{:S(2)}, u32[]{:S(2)}) async-start(f32[1,128,4]{1,0,2:T(1,128)} %broadcast_in_dim.19), calls=%async_computation | async-start | bytes 4096 | tf_op jit(solution)/shard_map/all_to_all | solution.py:38
  112.6 7.6 %fusion.9 = bf16[2048,128]{1,0:T(8,128)(2,1)} fusion(bf16[2048,128]{1,0:T(8,128)(2,1)} %param.11, f32[2048,128]{1,0:T(8,128)S(1)} %bitcast.43, f32[2048,128]{1,0:T(8,128)} %get-tuple-element.5, bf16[2048,2048]{1,0:T(8,128)(2,1)} %all-gather.2.cloned.1.call-done, f32[2048]{0:T(1024)S(1)} %copy-done.5, f32[2048]{0:T(1024)S(1)} %add_rsqrt_fusion), kind=kOutput, calls=%fused_computation.16 | convolution fusion | flops 1093926912 | bytes 11550720 | tf_op jit(solution)/shard_map/dot_general | solution.py:20
  120.2 0.0 copy-done
  120.2 0.0 copy-start.2
  120.2 10.2 %fusion.10 = f32[128,512]{0,1:T(8,128)} fusion(bf16[2048,128]{1,0:T(8,128)(2,1)} %fusion.9, bf16[2048,512]{1,0:T(8,128)(2,1)S(1)} %copy-done, bf16[2048,2048]{1,0:T(8,128)(2,1)} %all-gather.2.cloned.1.call-done, f32[2048]{0:T(1024)S(1)} %copy-done.5, f32[2048]{0:T(1024)S(1)} %add_rsqrt_fusion), kind=kOutput, calls=%fused_computation.17 | convolution fusion | flops 4581228544 | bytes 11288576 | tf_op jit(solution)/shard_map/dot_general | solution.py:29
  130.4 0.0 all-to-all-done
  130.5 4.2 %all-to-all-start.1 = ((f32[1,128,512]{1,0,2:T(1,128)}), f32[1,128,512]{1,0,2:T(1,128)S(1)}, u32[]{:S(2)}, u32[]{:S(2)}) async-start(f32[1,128,512]{1,0,2:T(1,128)} %bitcast.18), calls=%async_computation.1 | async-start | bytes 524288 | tf_op jit(solution)/shard_map/all_to_all | solution.py:37
  134.7 5.3 %all-to-all-done.1 = f32[1,128,512]{1,0,2:T(1,128)S(1)} async-done(((f32[1,128,512]{1,0,2:T(1,128)}), f32[1,128,512]{1,0,2:T(1,128)S(1)}, u32[]{:S(2)}, u32[]{:S(2)}) %all-to-all-start.1) | async-done | bytes 262176 | tf_op jit(solution)/shard_map/all_to_all | solution.py:37
  140.0 0.3 fusion.23
  140.3 13.6 %psum.14 = f32[4,128]{1,0:T(4,128)S(1)} all-reduce(f32[4,128]{1,0:T(4,128)S(1)} %fusion.23), channel_id=1, replica_groups=mesh['sp'=4,'tp'=8] {'tp'}, use_global_device_ids=true, to_apply=%region_5.6 | all-reduce | flops 512 | bytes 4096 | tf_op jit(solution)/shard_map/psum | solution.py:53
  153.9 0.1 multiply_reduce_fusion.1
  154.1 8.7 %psum.15 = f32[4]{0:T(128)S(1)} all-reduce(f32[4]{0:T(128)S(1)} %multiply_reduce_fusion.1), channel_id=1, replica_groups=mesh['sp'=4,'tp'=8] {'sp'}, use_global_device_ids=true, to_apply=%region_7.8 | all-reduce | flops 4 | bytes 32 | tf_op jit(solution)/shard_map/psum | solution.py:54
  162.8 0.7 copy.19
  163.5 0.0 copy-done.2
  163.5 0.6 multiply_multiply_fusion
  (11 shorter events, 0.1 us)
Async XLA Ops:
  7.2 113.1 %copy-start = (bf16[2048,512]{1,0:T(8,128)(2,1)S(1)}, bf16[2048,512]{1,0:T(8,128)(2,1)}, u32[]{:S(2)}) copy-start(bf16[2048,512]{1,0:T(8,128)(2,1)} %param.13) | copy-start | bytes 6291460
  7.2 92.9 %copy-start.5 = (f32[2048]{0:T(1024)S(1)}, f32[2048]{0:T(1024)}, u32[]{:S(2)}) copy-start(f32[2048]{0:T(1024)} %param.10) | copy-start | bytes 24580
  7.2 92.9 %copy-start.3 = (bf16[2048,128]{1,0:T(8,128)(2,1)S(1)}, bf16[2048,128]{1,0:T(8,128)(2,1)}, u32[]{:S(2)}) copy-start(bf16[2048,128]{1,0:T(8,128)(2,1)} %param.12) | copy-start | bytes 1572868
  7.2 92.9 %copy-start.6 = (f32[128]{0:T(128)S(1)}, f32[128]{0:T(128)}, u32[]{:S(2)}) copy-start(f32[128]{0:T(128)} %param.14) | copy-start | bytes 1540
  7.2 92.9 %copy-start.4 = (f32[2048]{0:T(1024)S(1)}, f32[2048]{0:T(1024)}, u32[]{:S(2)}) copy-start(f32[2048]{0:T(1024)} %param.15) | copy-start | bytes 24580
  7.2 87.6 %all-gather.2.cloned.1.call-start = ((), (), s32[]{:S(2)}) async-start(), calls=%async_computation.2 | async-start | bytes 9437184 | tf_op jit(solution)/shard_map/all_gather | solution.py:16
  94.9 5.8 %copy-start.1 = (bf16[2048,2048]{1,0:T(8,128)(2,1)S(1)}, bf16[2048,2048]{1,0:T(8,128)(2,1)}, u32[]{:S(2)}) copy-start(bf16[2048,2048]{1,0:T(8,128)(2,1)} %all-gather.2.cloned.1.call-done) | copy-start | bytes 25165828
  109.0 21.5 %all-to-all-start = ((f32[1,128,4]{1,0,2:T(1,128)}), f32[1,128,4]{1,0,2:T(1,128)S(1)}, u32[]{:S(2)}, u32[]{:S(2)}) async-start(f32[1,128,4]{1,0,2:T(1,128)} %broadcast_in_dim.19), calls=%async_computation | async-start | bytes 4096 | tf_op jit(solution)/shard_map/all_to_all | solution.py:38
  120.2 43.3 %copy-start.2 = (f32[4,128]{1,0:T(4,128)S(1)}, f32[4,128]{1,0:T(4,128)}, u32[]{:S(2)}) copy-start(f32[4,128]{1,0:T(4,128)} %param.17) | copy-start | bytes 6148
  130.5 9.6 %all-to-all-start.1 = ((f32[1,128,512]{1,0,2:T(1,128)}), f32[1,128,512]{1,0,2:T(1,128)S(1)}, u32[]{:S(2)}, u32[]{:S(2)}) async-start(f32[1,128,512]{1,0,2:T(1,128)} %bitcast.18), calls=%async_computation.1 | async-start | bytes 524288 | tf_op jit(solution)/shard_map/all_to_all | solution.py:37
Sparse Core Ops, SparseCore 0:
  9.6 85.1 all-gather.1
where the time goes:
time: 171 us
  waiting for transfers between devices  92.2 us (54%)
  matrix products  22.8 us (13%)
  blocking collectives  22.4 us (13%)
  between operations  14.2 us (8%)
  other arithmetic  9.45 us (6%)
  starting transfers between devices  7.88 us (5%)
  local copies, waits for them, and re-layouts  2.17 us (1%)
    all_gather x1, waiting for transfers between devices, body(): gathered = lax.all_gather(tokens, 'tp', axis=1, tiled=True)  86.2 us
    psum x1, blocking collectives, body(): summed_read = lax.psum(part_read, 'tp')  13.6 us
    dot_general x1, matrix products, body(): lax.dot_general(weighted, value_proj, (((0,), (0,)), ((), ())), preferred...  10.2 us
    psum x1, blocking collectives, body(): squares = lax.psum(jnp.sum(summed_read * summed_read, axis=1), 'sp')  8.74 us
    dot_general x1, matrix products, body(): jnp.dot(normed, w_key, preferred_element_type=jnp.float32)  7.58 us
    all_to_all x1, waiting for transfers between devices, body(): lax.all_to_all(partial_value[None], 'sp', split_axis=2, concat_axis=0, ti...  5.33 us
    reduce_sum x1, other arithmetic, body(): jnp.mean(rows_f32 * rows_f32, axis=1, keepdims=True) + EPS  5.23 us
    dot_general x1, matrix products, body(): jnp.dot(normed, w_decay, preferred_element_type=jnp.float32)  4.74 us
  transfers between devices with their start and end apart: 3, of which 2 were waited for; matrix products, arithmetic and copies ran while one was open for 11% of the time, Pallas kernels for 0%

commit v1 on v0

--- a/solution.py
+++ b/solution.py
@@ -1,6 +1,10 @@
+import functools
+
 import jax
 import jax.numpy as jnp
 from jax import lax
+from jax.experimental import pallas as pl
+from jax.experimental.pallas import tpu as pltpu
 from jax.sharding import PartitionSpec as P
 
 QUERY_KEY_HEADS = 4
@@ -56,9 +60,334 @@
     return (state_cache, first_read)
 
 
+PAIR = 2
+LANES = 128
+F32 = jnp.float32
+BF16 = jnp.bfloat16
+
+
+def dot(a, b):
+    return jnp.dot(a, b, preferred_element_type=F32)
+
+
+def kernel(n_sp, n_tp, query_scale, tokens, gain, wk, wd, wv, bias, drift, query, out_gain,
+           state_out, read_out,
+           tok, wbuf, wval, normed, val_t, biases, part_send, part_recv, tot_send, tot_recv, rd_send, rd_recv,
+           load_sem, tok_s, tok_r, half_s, half_r, wz_s, w_r, wp_s, bias_s, bias_r,
+           part_s, part_r, tot_s, tot_r, rd_s, rd_r):
+    nz = n_tp // PAIR
+    n = n_sp * n_tp
+    s, t = lax.axis_index("sp"), lax.axis_index("tp")
+    z, c = t // PAIR, t % PAIR
+    me = s * n_tp + t
+    rows = tok.shape[1]
+    quarter = wbuf.shape[1] // n_sp
+    vals = LANES
+
+    def remote(src, dst, ssem, rsem, sp, tp):
+        return pltpu.make_async_remote_copy(
+            src_ref=src, dst_ref=dst, send_sem=ssem, recv_sem=rsem,
+            device_id=(sp, tp), device_id_type=pl.DeviceIdType.MESH)
+
+    loads = [
+        pltpu.make_async_copy(wk, wbuf.at[z, :, 0:LANES], load_sem.at[0]),
+        pltpu.make_async_copy(wd, wbuf.at[z, :, LANES:2 * LANES], load_sem.at[1]),
+        pltpu.make_async_copy(wv, wval, load_sem.at[2]),
+    ]
+    for load in loads:
+        load.start()
+
+    barrier = pltpu.get_barrier_semaphore()
+
+    def greet(d, carry):
+        other = (me + d) % n
+        pl.semaphore_signal(barrier, inc=1, device_id=(other // n_tp, other % n_tp),
+                            device_id_type=pl.DeviceIdType.MESH)
+        return carry
+    lax.fori_loop(1, n, greet, 0)
+    loads[0].wait()
+    loads[1].wait()
+    pl.semaphore_wait(barrier, n - 1)
+
+    def w_slot(zo, q):
+        return wbuf.at[zo, pl.ds(pl.multiple_of(q * quarter, LANES), quarter), :]
+
+    def along(zo, dz, k):
+        side = (dz + 1) // 2
+        return remote(w_slot(zo, s), w_slot(zo, s), wz_s.at[side, k], w_r.at[zo, s],
+                      s, (z + dz) * PAIR + c)
+
+    def in_plane(zo, i):
+        return remote(w_slot(zo, s), w_slot(zo, s), wp_s.at[zo, i - 1], w_r.at[zo, s],
+                      (s + i) % n_sp, t)
+
+    def to_column(i):
+        zd = (z + i) % nz
+        return remote(tokens.at[pl.ds(pl.multiple_of(zd * rows, LANES), rows), :], tok.at[t],
+                      tok_s.at[i - 1], tok_r.at[t], s, zd * PAIR + c)
+
+    def bias_to(i):
+        return remote(bias, biases.at[z], bias_s.at[i - 1], bias_r.at[z], s, ((z + i) % nz) * PAIR + c)
+
+    def to_pair(zo):
+        return remote(tok.at[zo * PAIR + c], tok.at[zo * PAIR + c], half_s.at[zo],
+                      half_r.at[zo], s, z * PAIR + 1 - c)
+
+    for dz in (1, -1):
+        @pl.when((z + dz >= 0) & (z + dz < nz))
+        def _():
+            along(z, dz, 0).start()
+    tok_own = pltpu.make_async_copy(
+        tokens.at[pl.ds(pl.multiple_of(z * rows, LANES), rows), :], tok.at[t], load_sem.at[0])
+    tok_own.start()
+    for i in range(1, nz):
+        bias_to(i).start()
+    far = nz // 2
+    to_column(far).start()
+    biases[z] = bias[...]
+    tok_own.wait()
+    to_pair(z).start()
+
+    for k in range(1, nz):
+        for dz in (1, -1):
+            zo = z - k * dz
+
+            @pl.when((zo >= 0) & (zo < nz))
+            def _():
+                along(zo, dz, 0).wait_recv()
+
+                @pl.when((z + dz >= 0) & (z + dz < nz))
+                def _():
+                    along(zo, dz, k).start()
+                for i in range(1, n_sp):
+                    in_plane(zo, i).start()
+        if k == 1:
+            for i in range(1, nz):
+                if i != far:
+                    to_column(i).start()
+
+    for i in [far] + [i for i in range(1, nz) if i != far]:
+        zo = (z + nz - i) % nz
+        pltpu.make_async_copy(tok.at[zo * PAIR + c], tok.at[zo * PAIR + c], tok_r.at[zo * PAIR + c]).wait()
+        to_pair(zo).start()
+
+    def got_pair(zo):
+        other = zo * PAIR + 1 - c
+        pltpu.make_async_copy(tok.at[other], tok.at[other], half_r.at[zo]).wait()
+    for zo in range(nz):
+        got_pair(zo)
+
+    feats = tok.shape[2]
+    squares = jnp.zeros((rows, LANES), F32)
+    for b in range(n_tp):
+        x = tok[b].astype(F32)
+        for l in range(feats // LANES):
+            y = x[:, l * LANES:(l + 1) * LANES]
+            squares = squares + y * y
+    inverse = lax.rsqrt(jnp.sum(squares, axis=1, keepdims=True) / (n_tp * feats) + EPS)
+    for b in range(n_tp):
+        cols = slice(b * feats, (b + 1) * feats)
+        normed[:, cols] = (tok[b].astype(F32) * inverse * gain[:, cols]).astype(BF16)
+    loads[2].wait()
+    val_t[...] = dot(normed[...], wval[...]).T.astype(BF16)
+    drift_col = jnp.broadcast_to(drift[z], (LANES, rows)).T
+    tri = (lax.broadcasted_iota(jnp.int32, (rows, rows), 1)
+           > lax.broadcasted_iota(jnp.int32, (rows, rows), 0)).astype(BF16)
+
+    own = s * nz + z
+
+    def part_to(zo, sd):
+        return remote(part_send.at[zo, pl.ds(pl.multiple_of(sd * vals, vals), vals), :], part_recv.at[own],
+                      part_s.at[zo, sd], part_r.at[own], sd, zo * PAIR + c)
+
+    def tot_to(zo, sd):
+        return remote(tot_send.at[zo], tot_recv.at[own], tot_s.at[zo, sd], tot_r.at[own],
+                      sd, zo * PAIR + c)
+
+    for i in range(1, nz):
+        zo = (z + i) % nz
+        pltpu.make_async_copy(biases.at[zo], biases.at[zo], bias_r.at[zo]).wait()
+
+    def block(j, carry):
+        zo = (z + j) % nz
+
+        @pl.when(j > 0)
+        def _():
+            for i in range(1, n_sp):
+                q = (s + i) % n_sp
+                pltpu.make_async_copy(w_slot(zo, q), w_slot(zo, q), w_r.at[zo, q]).wait()
+        proj = dot(normed[...], wbuf[zo])
+        key = proj[:, :LANES].astype(BF16).astype(F32)
+        gate = proj[:, LANES:].astype(BF16).astype(F32)
+        u = gate + biases[zo] + drift_col
+        log_decay = (jnp.minimum(u, 0.0) - jnp.log1p(jnp.exp(-jnp.abs(u)))) / GATE_NORM
+        high = log_decay.astype(BF16)
+        low = (log_decay - high.astype(F32)).astype(BF16)
+        later = dot(tri, jnp.concatenate([high, low], axis=1))
+        rest = later[:, :LANES] + later[:, LANES:]
+        weighted = (key * jnp.exp(rest)).astype(BF16)
+        tot_send[zo] = jnp.sum(log_decay, axis=0, keepdims=True)
+        part_send[zo] = dot(val_t[...], weighted).astype(BF16)
+        for i in range(1, n_sp):
+            sd = (s + i) % n_sp
+            part_to(zo, sd).start()
+            tot_to(zo, sd).start()
+
+        @pl.when(j > 0)
+        def _():
+            part_to(zo, s).start()
+            tot_to(zo, s).start()
+        return carry
+    lax.fori_loop(0, nz, block, 0)
+    part_recv[own] = part_send[z, pl.ds(pl.multiple_of(s * vals, vals), vals), :]
+    tot_recv[own] = tot_send[z]
+
+    def arrived(d, carry):
+        src = (own + d) % (n_sp * nz)
+        pltpu.make_async_copy(part_recv.at[src], part_recv.at[src], part_r.at[src]).wait()
+        pltpu.make_async_copy(tot_recv.at[src], tot_recv.at[src], tot_r.at[src]).wait()
+        return carry
+    lax.fori_loop(1, n_sp * nz, arrived, 0)
+
+    later = jnp.zeros((1, LANES), F32)
+    total = jnp.zeros((vals, LANES), F32)
+    for k in reversed(range(n_sp * nz)):
+        total = total + jnp.exp(later) * part_recv[k].astype(F32)
+        later = later + tot_recv[k]
+    state_out[...] = total.T.astype(BF16)
+    scaled = query[...].astype(F32) * query_scale
+    rd_send[...] = jnp.sum((total * scaled).T, axis=0, keepdims=True)
+    rd_recv[me] = rd_send[...]
+
+    def read_to(d):
+        other = (me + d) % n
+        return remote(rd_send, rd_recv.at[me], rd_s.at[d], rd_r.at[me], other // n_tp, other % n_tp)
+
+    def send_read(d, carry):
+        read_to(d).start()
+        return carry
+    lax.fori_loop(1, n, send_read, 0)
+
+    for dz in (1, -1):
+        for k in range(nz - 1):
+            zo = z - k * dz
+
+            @pl.when((zo >= 0) & (zo < nz) & (z + dz >= 0) & (z + dz < nz))
+            def _():
+                along(zo, dz, k).wait_send()
+    for i in range(1, nz):
+        to_column(i).wait_send()
+        bias_to(i).wait_send()
+        for q in range(1, n_sp):
+            in_plane((z + i) % nz, q).wait_send()
+    for zo in range(nz):
+        to_pair(zo).wait_send()
+
+    def sent(j, carry):
+        zo = (z + j) % nz
+        for i in range(1, n_sp):
+            sd = (s + i) % n_sp
+            part_to(zo, sd).wait_send()
+            tot_to(zo, sd).wait_send()
+
+        @pl.when(j > 0)
+        def _():
+            part_to(zo, s).wait_send()
+            tot_to(zo, s).wait_send()
+        return carry
+    lax.fori_loop(0, nz, sent, 0)
+
+    def read_from(d, carry):
+        src = (me + d) % n
+        pltpu.make_async_copy(rd_recv.at[src], rd_recv.at[src], rd_r.at[src]).wait()
+        return carry
+    lax.fori_loop(1, n, read_from, 0)
+
+    def read_sent(d, carry):
+        read_to(d).wait_send()
+        return carry
+    lax.fori_loop(1, n, read_sent, 0)
+
+    heads = read_out.shape[0]
+    per_head = n_tp // heads
+
+    def head_row(sp, h):
+        row = rd_recv[sp * n_tp + h * per_head]
+        for i in range(1, per_head):
+            row = row + rd_recv[sp * n_tp + h * per_head + i]
+        return row
+    for h in range(heads):
+        squared = jnp.zeros((1, LANES), F32)
+        for sp in range(n_sp):
+            row = head_row(sp, h)
+            squared = squared + row * row
+        mean = jnp.sum(squared, axis=1, keepdims=True) / (n_sp * vals)
+        read_out[h:h + 1, :] = head_row(s, h) * lax.rsqrt(mean + EPS) * out_gain[h:h + 1, :]
+
+
+def fused_body(tokens, norm_gain, w_key, w_decay, w_value, decay_bias, gate_drift, queries, out_gain):
+    n_sp, n_tp = lax.axis_size("sp"), lax.axis_size("tp")
+    nz = n_tp // PAIR
+    span, feats = tokens.shape
+    width = feats * n_tp
+    rows = span // nz
+    channels = w_key.shape[1]
+    vals = out_gain.shape[1]
+    values = w_value.shape[1]
+    vmem = pl.BlockSpec(memory_space=pltpu.VMEM)
+    hbm = pl.BlockSpec(memory_space=pl.ANY)
+    dma = pltpu.SemaphoreType.DMA
+    return pl.pallas_call(
+        functools.partial(kernel, n_sp, n_tp, KEY_CHANNELS ** (-0.5)),
+        out_shape=(jax.ShapeDtypeStruct((channels, vals), BF16),
+                   jax.ShapeDtypeStruct(out_gain.shape, F32)),
+        in_specs=[vmem, vmem, hbm, hbm, hbm, vmem, vmem, vmem, vmem],
+        out_specs=(vmem, vmem),
+        scratch_shapes=[
+            pltpu.VMEM((n_tp, rows, feats), BF16),
+            pltpu.VMEM((nz, width, 2 * channels), BF16),
+            pltpu.VMEM((width, values), BF16),
+            pltpu.VMEM((rows, width), BF16),
+            pltpu.VMEM((values, rows), BF16),
+            pltpu.VMEM((nz, 1, channels), F32),
+            pltpu.VMEM((nz, values, channels), BF16),
+            pltpu.VMEM((n_sp * nz, vals, channels), BF16),
+            pltpu.VMEM((nz, 1, channels), F32),
+            pltpu.VMEM((n_sp * nz, 1, channels), F32),
+            pltpu.VMEM((1, vals), F32),
+            pltpu.VMEM((n_sp * n_tp, 1, vals), F32),
+            dma((3,)),
+            dma((nz - 1,)), dma((n_tp,)),
+            dma((nz,)), dma((nz,)),
+            dma((2, nz)), dma((nz, n_sp)), dma((nz, n_sp - 1)),
+            dma((nz - 1,)), dma((nz,)),
+            dma((nz, n_sp)), dma((n_sp * nz,)),
+            dma((nz, n_sp)), dma((n_sp * nz,)),
+            dma((n_sp * n_tp,)), dma((n_sp * n_tp,)),
+        ],
+        compiler_params=pltpu.CompilerParams(
+            collective_id=0, has_side_effects=True, vmem_limit_bytes=48 * 1024 * 1024),
+    )(tokens, norm_gain.reshape(1, width), w_key, w_decay, w_value, decay_bias.reshape(1, channels),
+      gate_drift.reshape(nz, 1, rows), queries.reshape(1, channels), out_gain)
+
+
+def fits(tokens, w_key, w_value, out_gain, n_tp):
+    nz = n_tp // PAIR
+    return (n_tp % PAIR == 0 and nz > 1 and tokens.shape[0] % (nz * LANES) == 0
+            and tokens.shape[1] % LANES == 0 and w_key.shape[1] == LANES and out_gain.shape[1] == LANES
+            and n_tp % out_gain.shape[0] == 0)
+
+
+def choose(tokens, norm_gain, w_key, w_decay, w_value, decay_bias, gate_drift, queries, out_gain):
+    args = (tokens, norm_gain, w_key, w_decay, w_value, decay_bias, gate_drift, queries, out_gain)
+    if fits(tokens, w_key, w_value, out_gain, lax.axis_size("tp")):
+        return fused_body(*args)
+    return body(*args)
+
+
 def solution(mesh):
     return jax.shard_map(
-        body,
+        choose,
         mesh=mesh,
         in_specs=(
             P("sp", "tp"),

time: 171 us -> 88.4 us (0.52)
  waiting for transfers between devices: 92.2 us -> 0 us
  Pallas kernels: 0 us -> 77.8 us
  matrix products: 22.8 us -> 0 us
  blocking collectives: 22.4 us -> 0 us
  between operations: 14.2 us -> 0.66 us
  other arithmetic: 9.45 us -> 0 us
  starting transfers between devices: 7.88 us -> 0 us
  local copies, waits for them, and re-layouts: 2.17 us -> 9.47 us
    all_gather x1 -> x0, waiting for transfers between devices: 86.2 us -> none  [body(): gathered = lax.all_gather(tokens, 'tp', axis=1, tiled=True)]
    pallas_call x0 -> x1, Pallas kernels: none -> 77.8 us  [fused_body(): pl.pallas_call(functools.partial(kernel, n_sp, n_tp, KEY_CHANNELS ** (-0....]
    dot_general x4 -> x0, matrix products: 22.8 us -> none  [the longest x1 10.2 us: body(): lax.dot_general(weighted, value_proj, (((0,), (0,)), ((), ())), preferred...]
    psum x2 -> x0, blocking collectives: 22.4 us -> none  [the longest x1 13.6 us: body(): summed_read = lax.psum(part_read, 'tp')]
    unnamed x15 -> x20, local copies, waits for them, and re-layouts: 1.24 us -> 9.47 us
    all_to_all x2 -> x0, starting transfers between devices: 7.84 us -> none  [the longest x1 4.19 us: body(): lax.all_to_all(partial_value[None], 'sp', split_axis=2, concat_axis=0, ti...]
    reduce_sum x3 -> x0, other arithmetic: 5.37 us -> none  [the longest x1 5.23 us: body(): jnp.mean(rows_f32 * rows_f32, axis=1, keepdims=True) + EPS]
    all_to_all x2 -> x0, waiting for transfers between devices: 5.33 us -> none  [the longest x1 5.33 us: body(): lax.all_to_all(partial_value[None], 'sp', split_axis=2, concat_axis=0, ti...]
  transfers between devices with their start and end apart: 3 -> 0, of which waited for: 2 -> 0; matrix products, arithmetic and copies ran while one was open for 11% -> 0% of each run, Pallas kernels for 0% -> 0%
where the time goes in v1:
time: 88.4 us; the launch traced here: 88 us
  Pallas kernels  77.8 us (88%)
  local copies, waits for them, and re-layouts  9.47 us (11%)
    pallas_call x1, Pallas kernels, fused_body(): pl.pallas_call(functools.partial(kernel, n_sp, n_tp, KEY_CHANNELS ** (-0....  77.8 us
    unnamed x20, local copies, waits for them, and re-layouts  9.47 us

profile of v1, /device:TPU:0, one launch (start us, length us, event | category | flops | bytes accessed | tf_op | source)
XLA Modules:
  0.0 88.0 jit_solution(18228080693037310007)
XLA Ops:
  0.6 0.0 copy-start
  0.6 1.6 %copy-done = bf16[2048,512]{1,0:T(8,128)(2,1)S(1)} copy-done((bf16[2048,512]{1,0:T(8,128)(2,1)S(1)}, bf16[2048,512]{1,0:T(8,128)(2,1)}, u32[]{:S(2)}) %copy-start) | copy-done | bytes 2097176
  2.2 0.0 copy-start.1
  2.2 1.2 %copy-done.1 = bf16[2048,256]{1,0:T(8,128)(2,1)S(1)} copy-done((bf16[2048,256]{1,0:T(8,128)(2,1)S(1)}, bf16[2048,256]{1,0:T(8,128)(2,1)}, u32[]{:S(2)}) %copy-start.1) | copy-done | bytes 1048600
  3.5 0.0 copy-start.2
  3.5 1.0 %copy-done.2 = bf16[2048,128]{1,0:T(8,128)(2,1)S(1)} copy-done((bf16[2048,128]{1,0:T(8,128)(2,1)S(1)}, bf16[2048,128]{1,0:T(8,128)(2,1)}, u32[]{:S(2)}) %copy-start.2) | copy-done | bytes 524312
  4.5 0.0 copy-start.3
  4.5 1.0 %copy-done.3 = bf16[2048,128]{1,0:T(8,128)(2,1)S(1)} copy-done((bf16[2048,128]{1,0:T(8,128)(2,1)S(1)}, bf16[2048,128]{1,0:T(8,128)(2,1)}, u32[]{:S(2)}) %copy-start.3) | copy-done | bytes 524312
  5.5 0.0 copy-start.4
  5.5 0.7 copy-done.4
  6.2 0.0 copy-start.5
  6.2 0.7 copy-done.5
  6.9 0.0 copy-start.6
  6.9 0.7 copy-done.6
  7.6 0.0 copy-start.7
  7.6 0.7 copy-done.7
  8.3 0.0 copy-start.8
  8.3 0.7 copy-done.8
  8.9 77.8 %shard_map.104 = (bf16[128,128]{1,0:T(8,128)(2,1)S(1)}, f32[4,128]{1,0:T(4,128)S(1)}) custom-call(bf16[2048,256]{1,0:T(8,128)(2,1)S(1)} %copy-done.1, f32[1,2048]{1,0:T(1,128)S(1)} %bitcast.4, bf16[2048,128]{1,0:T(8,128)(2,1)S(1)} %copy-done.2, bf16[2048,128]{1,0:T(8,128)(2,1)S(1)} %copy-done.3, bf16[2048,512]{1,0:T(8,128)(2,1)S(1)} %copy-done, ...), custom_call_target="tpu_custom_call" | custom-call | tf_op jit(solution)/shard_map/pallas_call | solution.py:340
  86.8 0.6 copy.13
  87.4 0.6 copy.14
Async XLA Ops:
  0.6 1.6 %copy-start = (bf16[2048,512]{1,0:T(8,128)(2,1)S(1)}, bf16[2048,512]{1,0:T(8,128)(2,1)}, u32[]{:S(2)}) copy-start(bf16[2048,512]{1,0:T(8,128)(2,1)} %wv.1) | copy-start | bytes 6291460
  2.2 1.2 %copy-start.1 = (bf16[2048,256]{1,0:T(8,128)(2,1)S(1)}, bf16[2048,256]{1,0:T(8,128)(2,1)}, u32[]{:S(2)}) copy-start(bf16[2048,256]{1,0:T(8,128)(2,1)} %tokens.1) | copy-start | bytes 3145732
  3.5 1.0 %copy-start.2 = (bf16[2048,128]{1,0:T(8,128)(2,1)S(1)}, bf16[2048,128]{1,0:T(8,128)(2,1)}, u32[]{:S(2)}) copy-start(bf16[2048,128]{1,0:T(8,128)(2,1)} %wk.1) | copy-start | bytes 1572868
  4.5 1.0 %copy-start.3 = (bf16[2048,128]{1,0:T(8,128)(2,1)S(1)}, bf16[2048,128]{1,0:T(8,128)(2,1)}, u32[]{:S(2)}) copy-start(bf16[2048,128]{1,0:T(8,128)(2,1)} %wd.1) | copy-start | bytes 1572868
  5.5 0.7 copy-start.4
  6.2 0.7 copy-start.5
  6.9 0.7 copy-start.6
  7.6 0.7 copy-start.7
  8.3 0.7 copy-start.8

commit v2 on v1

--- a/solution.py
+++ b/solution.py
@@ -62,6 +62,8 @@
 
 PAIR = 2
 LANES = 128
+PLANE = 4
+VMEM_BYTES = 67_000_000
 F32 = jnp.float32
 BF16 = jnp.bfloat16
 
@@ -70,9 +72,9 @@
     return jnp.dot(a, b, preferred_element_type=F32)
 
 
-def kernel(n_sp, n_tp, query_scale, tokens, gain, wk, wd, wv, bias, drift, query, out_gain,
+def kernel(n_sp, n_tp, query_scale, tokens_in, gain_in, wk, wd, wv, bias_in, drift_in, query_in, out_gain_in,
            state_out, read_out,
-           tok, wbuf, wval, normed, val_t, biases, part_send, part_recv, tot_send, tot_recv, rd_send, rd_recv,
+           tokens, gain, drift, query, out_gain, tok, wbuf, wval, normed, val_t, biases, part_send, part_recv, tot_send, tot_recv, rd_send, rd_recv,
            load_sem, tok_s, tok_r, half_s, half_r, wz_s, w_r, wp_s, bias_s, bias_r,
            part_s, part_r, tot_s, tot_r, rd_s, rd_r):
     nz = n_tp // PAIR
@@ -92,7 +94,13 @@
     loads = [
         pltpu.make_async_copy(wk, wbuf.at[z, :, 0:LANES], load_sem.at[0]),
         pltpu.make_async_copy(wd, wbuf.at[z, :, LANES:2 * LANES], load_sem.at[1]),
-        pltpu.make_async_copy(wv, wval, load_sem.at[2]),
+        pltpu.make_async_copy(tokens_in, tokens, load_sem.at[2]),
+        pltpu.make_async_copy(bias_in, biases.at[z], load_sem.at[3]),
+        pltpu.make_async_copy(gain_in, gain, load_sem.at[4]),
+        pltpu.make_async_copy(drift_in, drift, load_sem.at[5]),
+        pltpu.make_async_copy(query_in, query, load_sem.at[6]),
+        pltpu.make_async_copy(out_gain_in, out_gain, load_sem.at[7]),
+        pltpu.make_async_copy(wv, wval, load_sem.at[8]),
     ]
     for load in loads:
         load.start()
@@ -105,8 +113,8 @@
                             device_id_type=pl.DeviceIdType.MESH)
         return carry
     lax.fori_loop(1, n, greet, 0)
-    loads[0].wait()
-    loads[1].wait()
+    for load in loads[:4]:
+        load.wait()
     pl.semaphore_wait(barrier, n - 1)
 
     def w_slot(zo, q):
@@ -117,9 +125,25 @@
         return remote(w_slot(zo, s), w_slot(zo, s), wz_s.at[side, k], w_r.at[zo, s],
                       s, (z + dz) * PAIR + c)
 
+    x_bit, y_bit = s % 2, s // 2
+    x_peer, y_peer = y_bit * 2 + 1 - x_bit, (1 - y_bit) * 2 + x_bit
+    corner = (1 - y_bit) * 2 + 1 - x_bit
+    peers = (x_peer, y_peer)
+
     def in_plane(zo, i):
-        return remote(w_slot(zo, s), w_slot(zo, s), wp_s.at[zo, i - 1], w_r.at[zo, s],
-                      (s + i) % n_sp, t)
+        return remote(w_slot(zo, s), w_slot(zo, s), wp_s.at[zo, i], w_r.at[zo, s], peers[i], t)
+
+    def relay(zo, i):
+        half = quarter // 2
+        q = peers[1 - i]
+        part = wbuf.at[zo, pl.ds(pl.multiple_of(q * quarter + i * half, LANES), half), :]
+        return remote(part, part, wp_s.at[zo, 2 + i], w_r.at[zo, q], peers[i], t)
+
+    def relay_both(zo):
+        for i in range(2):
+            q = peers[1 - i]
+            pltpu.make_async_copy(w_slot(zo, q), w_slot(zo, q), w_r.at[zo, q]).wait()
+            relay(zo, i).start()
 
     def to_column(i):
         zd = (z + i) % nz
@@ -127,7 +151,7 @@
                       tok_s.at[i - 1], tok_r.at[t], s, zd * PAIR + c)
 
     def bias_to(i):
-        return remote(bias, biases.at[z], bias_s.at[i - 1], bias_r.at[z], s, ((z + i) % nz) * PAIR + c)
+        return remote(biases.at[z], biases.at[z], bias_s.at[i - 1], bias_r.at[z], s, ((z + i) % nz) * PAIR + c)
 
     def to_pair(zo):
         return remote(tok.at[zo * PAIR + c], tok.at[zo * PAIR + c], half_s.at[zo],
@@ -144,9 +168,16 @@
         bias_to(i).start()
     far = nz // 2
     to_column(far).start()
-    biases[z] = bias[...]
     tok_own.wait()
     to_pair(z).start()
+
+    def relay_step(k):
+        for dz in (1, -1):
+            zo = z - k * dz
+
+            @pl.when((zo >= 0) & (zo < nz))
+            def _():
+                relay_both(zo)
 
     for k in range(1, nz):
         for dz in (1, -1):
@@ -159,8 +190,10 @@
                 @pl.when((z + dz >= 0) & (z + dz < nz))
                 def _():
                     along(zo, dz, k).start()
-                for i in range(1, n_sp):
+                for i in range(2):
                     in_plane(zo, i).start()
+        if k > 1:
+            relay_step(k - 1)
         if k == 1:
             for i in range(1, nz):
                 if i != far:
@@ -177,6 +210,8 @@
     for zo in range(nz):
         got_pair(zo)
 
+    for load in loads[4:8]:
+        load.wait()
     feats = tok.shape[2]
     squares = jnp.zeros((rows, LANES), F32)
     for b in range(n_tp):
@@ -188,7 +223,8 @@
     for b in range(n_tp):
         cols = slice(b * feats, (b + 1) * feats)
         normed[:, cols] = (tok[b].astype(F32) * inverse * gain[:, cols]).astype(BF16)
-    loads[2].wait()
+    relay_step(nz - 1)
+    loads[8].wait()
     val_t[...] = dot(normed[...], wval[...]).T.astype(BF16)
     drift_col = jnp.broadcast_to(drift[z], (LANES, rows)).T
     tri = (lax.broadcasted_iota(jnp.int32, (rows, rows), 1)
@@ -208,14 +244,18 @@
         zo = (z + i) % nz
         pltpu.make_async_copy(biases.at[zo], biases.at[zo], bias_r.at[zo]).wait()
 
+    def nearest(j):
+        low = z < nz // 2
+        edge = jnp.where(low, z, nz - 1 - z)
+        at = jnp.where(j == 0, edge, jnp.where(j - 1 < edge, j - 1, j))
+        return jnp.where(low, at, nz - 1 - at)
+
     def block(j, carry):
-        zo = (z + j) % nz
+        zo = nearest(j)
 
         @pl.when(j > 0)
         def _():
-            for i in range(1, n_sp):
-                q = (s + i) % n_sp
-                pltpu.make_async_copy(w_slot(zo, q), w_slot(zo, q), w_r.at[zo, q]).wait()
+            pltpu.make_async_copy(w_slot(zo, corner), w_slot(zo, corner), w_r.at[zo, corner]).wait()
         proj = dot(normed[...], wbuf[zo])
         key = proj[:, :LANES].astype(BF16).astype(F32)
         gate = proj[:, LANES:].astype(BF16).astype(F32)
@@ -254,7 +294,6 @@
     for k in reversed(range(n_sp * nz)):
         total = total + jnp.exp(later) * part_recv[k].astype(F32)
         later = later + tot_recv[k]
-    state_out[...] = total.T.astype(BF16)
     scaled = query[...].astype(F32) * query_scale
     rd_send[...] = jnp.sum((total * scaled).T, axis=0, keepdims=True)
     rd_recv[me] = rd_send[...]
@@ -267,6 +306,7 @@
         read_to(d).start()
         return carry
     lax.fori_loop(1, n, send_read, 0)
+    state_out[...] = total.T.astype(BF16)
 
     for dz in (1, -1):
         for k in range(nz - 1):
@@ -278,13 +318,14 @@
     for i in range(1, nz):
         to_column(i).wait_send()
         bias_to(i).wait_send()
-        for q in range(1, n_sp):
-            in_plane((z + i) % nz, q).wait_send()
+        for j in range(2):
+            in_plane((z + i) % nz, j).wait_send()
+            relay((z + i) % nz, j).wait_send()
     for zo in range(nz):
         to_pair(zo).wait_send()
 
     def sent(j, carry):
-        zo = (z + j) % nz
+        zo = nearest(j)
         for i in range(1, n_sp):
             sd = (s + i) % n_sp
             part_to(zo, sd).wait_send()
@@ -335,15 +376,20 @@
     vals = out_gain.shape[1]
     values = w_value.shape[1]
     vmem = pl.BlockSpec(memory_space=pltpu.VMEM)
-    hbm = pl.BlockSpec(memory_space=pl.ANY)
+    hbm = pl.BlockSpec(memory_space=pltpu.HBM)
     dma = pltpu.SemaphoreType.DMA
     return pl.pallas_call(
         functools.partial(kernel, n_sp, n_tp, KEY_CHANNELS ** (-0.5)),
         out_shape=(jax.ShapeDtypeStruct((channels, vals), BF16),
                    jax.ShapeDtypeStruct(out_gain.shape, F32)),
-        in_specs=[vmem, vmem, hbm, hbm, hbm, vmem, vmem, vmem, vmem],
+        in_specs=[hbm] * 9,
         out_specs=(vmem, vmem),
         scratch_shapes=[
+            pltpu.VMEM(tokens.shape, BF16),
+            pltpu.VMEM((1, width), F32),
+            pltpu.VMEM((nz, 1, rows), F32),
+            pltpu.VMEM((1, channels), BF16),
+            pltpu.VMEM(out_gain.shape, F32),
             pltpu.VMEM((n_tp, rows, feats), BF16),
             pltpu.VMEM((nz, width, 2 * channels), BF16),
             pltpu.VMEM((width, values), BF16),
@@ -356,24 +402,24 @@
             pltpu.VMEM((n_sp * nz, 1, channels), F32),
             pltpu.VMEM((1, vals), F32),
             pltpu.VMEM((n_sp * n_tp, 1, vals), F32),
-            dma((3,)),
+            dma((9,)),
             dma((nz - 1,)), dma((n_tp,)),
             dma((nz,)), dma((nz,)),
-            dma((2, nz)), dma((nz, n_sp)), dma((nz, n_sp - 1)),
+            dma((2, nz)), dma((nz, n_sp)), dma((nz, 4)),
             dma((nz - 1,)), dma((nz,)),
             dma((nz, n_sp)), dma((n_sp * nz,)),
             dma((nz, n_sp)), dma((n_sp * nz,)),
             dma((n_sp * n_tp,)), dma((n_sp * n_tp,)),
         ],
         compiler_params=pltpu.CompilerParams(
-            collective_id=0, has_side_effects=True, vmem_limit_bytes=48 * 1024 * 1024),
+            collective_id=0, has_side_effects=True, vmem_limit_bytes=VMEM_BYTES),
     )(tokens, norm_gain.reshape(1, width), w_key, w_decay, w_value, decay_bias.reshape(1, channels),
       gate_drift.reshape(nz, 1, rows), queries.reshape(1, channels), out_gain)
 
 
 def fits(tokens, w_key, w_value, out_gain, n_tp):
     nz = n_tp // PAIR
-    return (n_tp % PAIR == 0 and nz > 1 and tokens.shape[0] % (nz * LANES) == 0
+    return (lax.axis_size("sp") == PLANE and n_tp % PAIR == 0 and nz > 1 and tokens.shape[0] % (nz * LANES) == 0
             and tokens.shape[1] % LANES == 0 and w_key.shape[1] == LANES and out_gain.shape[1] == LANES
             and n_tp % out_gain.shape[0] == 0)
 

time: 88.4 us -> 78.4 us (0.89)
  local copies, waits for them, and re-layouts: 9.47 us -> 2.62 us
  Pallas kernels: 77.8 us -> 75 us
    unnamed x20 -> x2, local copies, waits for them, and re-layouts: 9.47 us -> 2.62 us
    pallas_call x1, Pallas kernels: 77.8 us -> 75 us  [fused_body(): pl.pallas_call(functools.partial(kernel, n_sp, n_tp, KEY_CHANNELS ** (-0....]
where the time goes in v2:
time: 78.4 us; the launch traced here: 78.2 us
  Pallas kernels  75 us (96%)
  local copies, waits for them, and re-layouts  2.62 us (3%)
    pallas_call x1, Pallas kernels, fused_body(): pl.pallas_call(functools.partial(kernel, n_sp, n_tp, KEY_CHANNELS ** (-0....  75 us
    unnamed x2, local copies, waits for them, and re-layouts  2.62 us

profile of v2, /device:TPU:0, one launch (start us, length us, event | category | flops | bytes accessed | tf_op | source)
XLA Modules:
  0.0 78.2 jit_solution(3936209465892596262)
XLA Ops:
  0.6 75.0 %shard_map.104 = (bf16[128,128]{1,0:T(8,128)(2,1)}, f32[4,128]{1,0:T(4,128)}) custom-call(bf16[2048,256]{1,0:T(8,128)(2,1)} %tokens_in.1, f32[1,2048]{1,0:T(1,128)} %bitcast.4, bf16[2048,128]{1,0:T(8,128)(2,1)} %wk.1, bf16[2048,128]{1,0:T(8,128)(2,1)} %wd.1, bf16[2048,512]{1,0:T(8,128)(2,1)} %wv.1, f32[1,128]{1,0:T(1,128)} %bitcast.6, f32[4,1,512]{2,1,0:T(1,128)} %bitcast.5, ...), custom_call_target="tpu_custom_call" | custom-call | tf_op jit(solution)/shard_map/pallas_call | solution.py:381
  75.6 1.4 %copy.13 = bf16[128,128]{1,0:T(8,128)(2,1)} copy(bf16[128,128]{1,0:T(8,128)(2,1)} %get-tuple-element.4) | data formatting | bytes 65536
  77.0 1.2 %copy.14 = f32[4,128]{1,0:T(4,128)} copy(f32[4,128]{1,0:T(4,128)} %get-tuple-element.5) | data formatting | bytes 4096

commit v3 on v2

--- a/solution.py
+++ b/solution.py
@@ -180,6 +180,8 @@
                 relay_both(zo)
 
     for k in range(1, nz):
+        if k > 1:
+            relay_step(k - 1)
         for dz in (1, -1):
             zo = z - k * dz
 
@@ -192,8 +194,6 @@
                     along(zo, dz, k).start()
                 for i in range(2):
                     in_plane(zo, i).start()
-        if k > 1:
-            relay_step(k - 1)
         if k == 1:
             for i in range(1, nz):
                 if i != far:

time: 78.4 us -> 77 us (0.982)
  Pallas kernels: 75 us -> 73.5 us
    pallas_call x1, Pallas kernels: 75 us -> 73.5 us  [fused_body(): pl.pallas_call(functools.partial(kernel, n_sp, n_tp, KEY_CHANNELS ** (-0....]
where the time goes in v3:
time: 77 us; the launch traced here: 76.8 us
  Pallas kernels  73.5 us (95%)
  local copies, waits for them, and re-layouts  2.62 us (3%)
    pallas_call x1, Pallas kernels, fused_body(): pl.pallas_call(functools.partial(kernel, n_sp, n_tp, KEY_CHANNELS ** (-0....  73.5 us
    unnamed x2, local copies, waits for them, and re-layouts  2.62 us

profile of v3, /device:TPU:0, one launch (start us, length us, event | category | flops | bytes accessed | tf_op | source)
XLA Modules:
  0.0 76.8 jit_solution(15992927698753944542)
XLA Ops:
  0.6 73.5 %shard_map.104 = (bf16[128,128]{1,0:T(8,128)(2,1)}, f32[4,128]{1,0:T(4,128)}) custom-call(bf16[2048,256]{1,0:T(8,128)(2,1)} %tokens_in.1, f32[1,2048]{1,0:T(1,128)} %bitcast.4, bf16[2048,128]{1,0:T(8,128)(2,1)} %wk.1, bf16[2048,128]{1,0:T(8,128)(2,1)} %wd.1, bf16[2048,512]{1,0:T(8,128)(2,1)} %wv.1, f32[1,128]{1,0:T(1,128)} %bitcast.6, f32[4,1,512]{2,1,0:T(1,128)} %bitcast.5, ...), custom_call_target="tpu_custom_call" | custom-call | tf_op jit(solution)/shard_map/pallas_call | solution.py:381
  74.2 1.4 %copy.13 = bf16[128,128]{1,0:T(8,128)(2,1)} copy(bf16[128,128]{1,0:T(8,128)(2,1)} %get-tuple-element.4) | data formatting | bytes 65536
  75.5 1.2 %copy.14 = f32[4,128]{1,0:T(4,128)} copy(f32[4,128]{1,0:T(4,128)} %get-tuple-element.5) | data formatting | bytes 4096
